TPU v7x, 32 devices: a whole 2x2x4 slice. The times are simulated.
32 devices in a mesh: sp: 8 (over z, y), tp: 4 (over x, core).
Axes of the slice: x: 2, y: 2, z: 4, core: 2. Of those that a mesh axis runs over, the one named last changes fastest.
Arguments:
- residual: bfloat16 [8192, 2048], P('sp'), may hold values from -8 to 8
- query_wide: bfloat16 [8192, 1024], P('sp', 'tp'), may hold values from -6 to 6
- key_wide: bfloat16 [8192, 1024], P('sp', 'tp'), may hold values from -6 to 6
- value_wide: bfloat16 [8192, 2048], P('sp', 'tp'), may hold values from -6 to 6
- decay_wide: bfloat16 [8192, 1024], P('sp', 'tp'), may hold values from -12 to 12
- gate_wide: bfloat16 [8192, 2048], P('sp', 'tp'), may hold values from -6 to 6
- query_narrow: bfloat16 [8192, 512], P('sp', 'tp'), may hold values from -6 to 6
- key_narrow: bfloat16 [8192, 512], P('sp', 'tp'), may hold values from -6 to 6
- value_narrow: bfloat16 [8192, 2048], P('sp', 'tp'), may hold values from -6 to 6
- decay_narrow: bfloat16 [8192, 512], P('sp', 'tp'), may hold values from -12 to 12
- gate_narrow: bfloat16 [8192, 2048], P('sp', 'tp'), may hold values from -6 to 6
- head_gain: float32 [512], replicated, may hold values from 0.1 to 1.9
- out_wide: bfloat16 [2048, 2048], P('tp'), may hold values from -0.125 to 0.125
- out_narrow: bfloat16 [2048, 2048], P('tp'), may hold values from -0.125 to 0.125
- mlp_gain: float32 [2048], replicated, may hold values from 0.1 to 1.9
- up_weight: bfloat16 [2048, 4096], P('sp', 'tp'), may hold values from -0.125 to 0.125
- down_weight: bfloat16 [4096, 2048], P('tp', 'sp'), may hold values from -0.09375 to 0.09375
Outputs:
- layer_out: bfloat16 [8192, 2048], P('sp', 'tp')
All inputs are finite; a program needn't handle non-finite values.
Results may differ from a plain program's by a relative error of at most 0.017.
Values may be sent and summed in bfloat16 or wider, within the bound.
A program may use at most 128 MiB of HBM per device.

v0:
```python
import jax
import jax.numpy as jnp
from jax import lax
from jax.sharding import PartitionSpec as P

HEADS = 4
BLOCK = 64
EPS = 1e-05
DECAY_NORMALIZER = 16.0
HIGHEST = lax.Precision.HIGHEST


def entering(array, axis, join, neutral):
    place = lax.axis_index(axis)
    gathered = jax.tree.map(
        lambda a, kind: lax.all_gather(a.astype(kind), axis),
        array,
        (jnp.bfloat16, jnp.bfloat16, jnp.bfloat16, jnp.bfloat16),
    )
    state = jax.tree.map(lambda a, e: jnp.zeros_like(a) + jnp.asarray(e, a.dtype), array, neutral)

    def one(step, state):
        return join(
            state,
            jax.tree.map(
                lambda a, own: lax.dynamic_index_in_dim(a, step, 0, False).astype(own.dtype),
                gathered,
                array,
            ),
        )

    return lax.fori_loop(0, place, one, state)


def block_pass(queries, keys_in, values_in, log_decay, block_len):
    num_blocks = queries.shape[0] // block_len

    def to_blocks(stacked):
        return stacked.reshape((num_blocks, block_len) + stacked.shape[1:])

    causal = jnp.tril(jnp.ones((block_len, block_len), dtype=bool))
    initial = (
        jnp.zeros((queries.shape[1], queries.shape[2], values_in.shape[2]), jnp.float32),
        jnp.zeros((queries.shape[1], queries.shape[2]), jnp.float32),
    )

    def advance(running, inputs):
        memory, offset = running
        block_q, block_k, block_v, block_g = inputs
        within = jnp.cumsum(block_g, axis=0)
        final_log = within[-1]
        scaled_q = block_q * jnp.exp(within)
        scaled_k = block_k * jnp.exp(-within)
        outside = jnp.einsum("ihd,hde->ihe", scaled_q, memory, precision=HIGHEST)
        scores = jnp.einsum("ihd,jhd->hij", scaled_q, scaled_k, precision=HIGHEST)
        scores = jnp.where(causal[None], scores, 0.0)
        inside = jnp.einsum("hij,jhe->ihe", scores, block_v, precision=HIGHEST)
        decayed_keys = scaled_k * jnp.exp(final_log)[None]
        memory = jnp.exp(final_log)[..., None] * memory + jnp.einsum(
            "jhd,jhe->hde", decayed_keys, block_v, precision=HIGHEST
        )
        carried_q = scaled_q * jnp.exp(offset)[None]
        return ((memory, offset + final_log), (outside + inside, carried_q))

    (memory, totals), (outputs, carried_q) = lax.scan(
        advance,
        initial,
        (to_blocks(queries), to_blocks(keys_in), to_blocks(values_in), to_blocks(log_decay)),
    )
    return (outputs.reshape(values_in.shape), carried_q.reshape(queries.shape), totals, memory)


def prepare(query, key_proj, value, decay, heads_here):
    row_count = query.shape[0]
    key_width = query.shape[1] // heads_here
    queries = query.astype(jnp.float32).reshape(row_count, heads_here, key_width) * key_width ** (
        -0.5
    )
    keys_in = key_proj.astype(jnp.float32).reshape(row_count, heads_here, key_width)
    values_in = value.astype(jnp.float32).reshape(
        row_count, heads_here, value.shape[1] // heads_here
    )
    log_decay = (
        jax.nn.log_sigmoid(decay.astype(jnp.float32)).reshape(row_count, heads_here, key_width)
        / DECAY_NORMALIZER
    )
    return (queries, keys_in, values_in, log_decay)


def finish(outputs, gate, head_gain):
    scale = lax.rsqrt(jnp.mean(jnp.square(outputs), axis=-1, keepdims=True) + EPS)
    gated = (
        outputs * scale * head_gain * jax.nn.silu(gate.astype(jnp.float32).reshape(outputs.shape))
    )
    return gated.reshape(outputs.shape[0], -1).astype(jnp.bfloat16)


def combine_states(earlier, later):
    return (
        earlier[0] + later[0],
        jnp.exp(later[0])[..., None] * earlier[1] + later[1],
        earlier[2] + later[2],
        jnp.exp(later[2])[..., None] * earlier[3] + later[3],
    )


def body(
    residual,
    query_wide,
    key_wide,
    value_wide,
    decay_wide,
    gate_wide,
    query_narrow,
    key_narrow,
    value_narrow,
    decay_narrow,
    gate_narrow,
    head_gain,
    out_wide,
    out_narrow,
    mlp_gain,
    up_weight,
    down_weight,
):
    heads_here = HEADS // lax.axis_size("tp")
    up_whole, down_whole = (
        lax.all_gather(up_weight, "sp", axis=0, tiled=True),
        lax.all_gather(down_weight, "sp", axis=1, tiled=True),
    )
    wq, wk, wv, wg = prepare(query_wide, key_wide, value_wide, decay_wide, heads_here)
    wide_out, wide_q, wide_total, wide_memory = block_pass(wq, wk, wv, wg, BLOCK)
    nq, nk, nv, ng = prepare(query_narrow, key_narrow, value_narrow, decay_narrow, heads_here)
    narrow_out, narrow_q, narrow_total, narrow_memory = block_pass(nq, nk, nv, ng, BLOCK)
    identity = (
        jnp.zeros_like(wide_total),
        jnp.zeros_like(wide_memory),
        jnp.zeros_like(narrow_total),
        jnp.zeros_like(narrow_memory),
    )
    incoming = entering(
        (wide_total, wide_memory, narrow_total, narrow_memory), "sp", combine_states, identity
    )
    wide_out = wide_out + jnp.einsum("ihd,hde->ihe", wide_q, incoming[1], precision=HIGHEST)
    narrow_out = narrow_out + jnp.einsum("ihd,hde->ihe", narrow_q, incoming[3], precision=HIGHEST)
    gated_wide = finish(wide_out, gate_wide, head_gain)
    gated_narrow = finish(narrow_out, gate_narrow, head_gain)
    head_terms = jnp.dot(gated_wide, out_wide, preferred_element_type=jnp.float32) + jnp.dot(
        gated_narrow, out_narrow, preferred_element_type=jnp.float32
    )
    tp_index = lax.axis_index("tp")
    col_count = residual.shape[1] // lax.axis_size("tp")
    full_width = residual.shape[1]
    residual_cols = lax.dynamic_slice_in_dim(residual, tp_index * col_count, col_count, 1)
    mixed_cols = lax.psum_scatter(
        head_terms.astype(jnp.bfloat16), "tp", scatter_dimension=1, tiled=True
    ).astype(jnp.float32)
    stream_cols = (residual_cols.astype(jnp.float32) + mixed_cols).astype(jnp.bfloat16)
    stream_f = stream_cols.astype(jnp.float32)
    squares = lax.psum(jnp.sum(jnp.square(stream_f), axis=1, keepdims=True), "tp")
    gain_cols = lax.dynamic_slice_in_dim(mlp_gain, tp_index * col_count, col_count, 0)
    normed_cols = (stream_f * lax.rsqrt(squares / full_width + EPS) * gain_cols).astype(
        jnp.bfloat16
    )
    normed = lax.all_gather(normed_cols, "tp", axis=1, tiled=True)
    before_activation = jnp.dot(normed, up_whole, preferred_element_type=jnp.float32)
    hidden = jnp.square(jax.nn.relu(before_activation)).astype(jnp.bfloat16)
    down_terms = jnp.dot(hidden, down_whole, preferred_element_type=jnp.float32)
    mlp_cols = lax.psum_scatter(
        down_terms.astype(jnp.bfloat16), "tp", scatter_dimension=1, tiled=True
    ).astype(jnp.float32)
    return (stream_cols.astype(jnp.float32) + mlp_cols).astype(jnp.bfloat16)


def solution(mesh):
    return jax.shard_map(
        body,
        mesh=mesh,
        in_specs=(
            P("sp", None),
            P("sp", "tp"),
            P("sp", "tp"),
            P("sp", "tp"),
            P("sp", "tp"),
            P("sp", "tp"),
            P("sp", "tp"),
            P("sp", "tp"),
            P("sp", "tp"),
            P("sp", "tp"),
            P("sp", "tp"),
            P(),
            P("tp", None),
            P("tp", None),
            P(),
            P("sp", "tp"),
            P("tp", "sp"),
        ),
        out_specs=P("sp", "tp"),
        check_vma=False,
    )
```

profile of v0, /device:TPU:0, one launch (start us, length us, event | category | flops | bytes accessed | tf_op | source)
XLA Modules:
  0.0 591.7 jit_solution(7153783925277661843)
XLA Ops:
  6.6 5.0 reshape.501
  15.4 68.5 %while.51 = (s32[]{:T(128)}, f32[1,128,512]{2,1,0:T(8,128)S(1)}, f32[1,128]{1,0:T(1,128)S(1)}, f32[16,64,1,512]{3,1,2,0:T(8,128)}, f32[16,64,1,128]{3,1,2,0:T(8,...) while((s32[]{:T(128)}, f32[1,128,512]{2,1,0:T(8,128)S(1)}, ...), condition=%wide.region_5.6_spmd.clone, body=%wide.region_3.5_spmd.clone.sunk | while | flops 133005568 | bytes 2333321 | solution.py:65
  84.7 2.7 fusion.81
  87.3 3.3 reshape.486
  91.6 3.3 reshape.487
  95.0 4.9 reshape.499
  99.8 2.0 reshape.498
  103.4 108.7 %while.50 = (s32[]{:T(128)}, f32[1,256,512]{2,1,0:T(8,128)S(1)}, f32[1,256]{1,0:T(1,128)S(1)}, f32[16,64,1,512]{3,1,2,0:T(8,128)}, f32[16,64,1,256]{3,1,2,0:T(8,...) while((s32[]{:T(128)}, f32[1,256,512]{2,1,0:T(8,128)S(1)}, ...), condition=%wide.region_2.3_spmd.clone, body=%wide.region_0.2_spmd.clone.sunk | while | flops 240787968 | bytes 3648133 | solution.py:65
  212.9 3.0 copy.32
  217.2 3.0 copy.34
  221.5 22.3 %all-gather.5 = bf16[8,1,128]{2,1,0:T(2,128)(2,1)S(1)} all-gather(bf16[1,1,128]{2,1,0:T(2,128)(2,1)S(1)} %convert_bitcast_fusion.1), channel_id=4, replica_groups=mesh['sp'=8,'tp'=4] {'sp'}, dimensions={0}, use_global_device_ids=true | all-gather | bytes 2304 | tf_op jit(solution)/shard_map/all_gather | solution.py:16
  243.9 16.7 %all-gather.4 = bf16[8,1,256]{2,1,0:T(2,128)(2,1)S(1)} all-gather(bf16[1,1,256]{2,1,0:T(2,128)(2,1)S(1)} %convert_bitcast_fusion), channel_id=2, replica_groups=mesh['sp'=8,'tp'=4] {'sp'}, dimensions={0}, use_global_device_ids=true | all-gather | bytes 4608 | tf_op jit(solution)/shard_map/all_gather | solution.py:16
  260.6 4.6 all-gather.18.cloned.1.call-done
  265.4 5.6 multiply_reduce_fusion.1
  273.2 2.8 fusion.78
  276.0 5.0 add_convert_fusion
  283.0 56.4 %reduce-scatter.3.cloned.1.call-done = bf16[1024,512]{1,0:T(8,128)(2,1)} async-done(((bf16[1024,2048]{1,0:T(8,128)(2,1)}), bf16[1024,512]{1,0:T(8,128)(2,1)}) %reduce-scatter.3.cloned.1.call-update) | async-done | bytes 1048592 | tf_op jit(solution)/shard_map/reduce_scatter | solution.py:155
  341.4 5.8 psum.7
  348.8 65.5 %all-gather.14.cloned.1.call-done = bf16[2048,1024]{1,0:T(8,128)(2,1)} async-done(((bf16[256,1024]{1,0:T(8,128)(2,1)}), bf16[2048,1024]{1,0:T(8,128)(2,1)}) %all-gather.14.cloned.1.call-update) | async-done | bytes 4194320 | tf_op jit(solution)/shard_map/all_gather | solution.py:128
  414.3 75.1 %all-gather.16.cloned.1.call-done = bf16[1024,2048]{1,0:T(8,128)(2,1)} async-done(((bf16[1024,256]{1,0:T(8,128)(2,1)}), bf16[1024,2048]{1,0:T(8,128)(2,1)}) %all-gather.16.cloned.1.call-update) | async-done | bytes 4194320 | tf_op jit(solution)/shard_map/all_gather | solution.py:129
  489.4 34.1 %all-gather.12.cloned.1.call-done = bf16[1024,2048]{1,0:T(8,128)(2,1)} async-done(((bf16[1024,512]{1,0:T(8,128)(2,1)}), bf16[1024,2048]{1,0:T(8,128)(2,1)}) %all-gather.12.cloned.1.call-update) | async-done | bytes 4194320 | tf_op jit(solution)/shard_map/all_gather | solution.py:165
  523.4 14.4 %convolution_convert_fusion = bf16[1024,2048]{1,0:T(8,128)(2,1)} fusion(bf16[1024,2048]{1,0:T(8,128)(2,1)} %all-gather.16.cloned.1.call-done, bf16[1024,2048]{1,0:T(8,128)(2,1)} %all-gather.12.cloned.1.call-done, bf16[2048,1024]{1,0:T(8,128)(2,1)} %all-gather.14.cloned.1.call-done), kind=kOutput, calls=%fused_computation.91 | convolution fusion | flops 8595177472 | bytes 16777216 | tf_op jit(solution)/shard_map/dot_general | solution.py:168
  537.9 44.5 %reduce-scatter.5.cloned.1.call-done = bf16[1024,512]{1,0:T(8,128)(2,1)} async-done(((bf16[1024,2048]{1,0:T(8,128)(2,1)}), bf16[1024,512]{1,0:T(8,128)(2,1)}) %reduce-scatter.5.cloned.1.call-update) | async-done | bytes 1048592 | tf_op jit(solution)/shard_map/reduce_scatter | solution.py:169
  582.4 2.5 fusion.74
  (423 shorter events, 193.9 us)
Async XLA Ops:
  6.5 266.6 %copy-start = (bf16[512,2048]{1,0:T(8,128)(2,1)S(1)}, bf16[512,2048]{1,0:T(8,128)(2,1)}, u32[]{:S(2)}) copy-start(bf16[512,2048]{1,0:T(8,128)(2,1)} %param.35) | copy-start | bytes 6291460
  6.5 5.0 copy-start.10
  6.5 5.1 copy-start.11
  6.5 254.0 %all-gather.20.cloned.1.call-start = ((), (), s32[]{:S(2)}) async-start(), calls=%async_computation.8 | async-start | bytes 1179648 | tf_op jit(solution)/shard_map/all_gather | solution.py:16
  83.9 6.7 %copy-start.7 = (bf16[1024,256]{1,0:T(8,128)(2,1)S(1)}, bf16[1024,256]{1,0:T(8,128)(2,1)}, u32[]{:S(2)}) copy-start(bf16[1024,256]{1,0:T(8,128)(2,1)} %param.24) | copy-start | bytes 1572868
  84.6 180.5 %all-gather.18.cloned.1.call-start = ((), (), s32[]{:S(2)}) async-start(), calls=%async_computation.7 | async-start | bytes 2359296 | tf_op jit(solution)/shard_map/all_gather | solution.py:16
  91.6 8.2 %copy-start.8 = (bf16[1024,256]{1,0:T(8,128)(2,1)S(1)}, bf16[1024,256]{1,0:T(8,128)(2,1)}, u32[]{:S(2)}) copy-start(bf16[1024,256]{1,0:T(8,128)(2,1)} %param.25) | copy-start | bytes 1572868
  212.9 126.6 %reduce-scatter.3.cloned.1.call-start = ((), (), s32[]{:S(2)}) async-start(), calls=%async_computation.2 | async-start | bytes 5242880 | tf_op jit(solution)/shard_map/reduce_scatter | solution.py:155
  212.9 3.0 copy-start.3
  217.2 3.0 copy-start.4
  265.4 5.7 copy-start.2
  265.4 5.7 copy-start.9
  271.1 2.1 copy-start.6
  271.1 2.1 copy-start.13
  273.2 2.8 copy-start.5
  273.2 2.8 copy-start.12
  281.0 133.2 %all-gather.14.cloned.1.call-start = ((), (), s32[]{:S(2)}) async-start(), calls=%async_computation.4 | async-start | bytes 4718592 | tf_op jit(solution)/shard_map/all_gather | solution.py:128
  281.6 207.7 %all-gather.16.cloned.1.call-start = ((), (), s32[]{:S(2)}) async-start(), calls=%async_computation.5 | async-start | bytes 4718592 | tf_op jit(solution)/shard_map/all_gather | solution.py:129
  282.2 241.2 %all-gather.12.cloned.1.call-start = ((), (), s32[]{:S(2)}) async-start(), calls=%async_computation.3 | async-start | bytes 5242880 | tf_op jit(solution)/shard_map/all_gather | solution.py:165
  348.5 233.9 %reduce-scatter.5.cloned.1.call-start = ((), (), s32[]{:S(2)}) async-start(), calls=%async_computation.6 | async-start | bytes 5242880 | tf_op jit(solution)/shard_map/reduce_scatter | solution.py:169
  537.9 47.0 %copy-start.1 = (bf16[512,2048]{1,0:T(8,128)(2,1)S(1)}, bf16[512,2048]{1,0:T(8,128)(2,1)}, u32[]{:S(2)}) copy-start(bf16[512,2048]{1,0:T(8,128)(2,1)} %param.35) | copy-start | bytes 6291460
Sparse Core Ops, SparseCore 0:
  84.7 43.0 all-gather.19
  213.0 52.1 all-gather.17
  281.2 58.2 reduce-scatter.2
  341.4 72.7 all-gather.13
  416.2 73.1 all-gather.15
  490.8 32.6 all-gather.11
  538.0 44.3 reduce-scatter.4
where the time goes:
time: 596 us; the launch traced here: 592 us
  waiting for transfers between devices  281 us (47%)
  matrix products  95.3 us (16%)
  local copies, waits for them, and re-layouts  83 us (14%)
  other arithmetic  71.2 us (12%)
  blocking collectives  44.8 us (8%)
  between operations  13.8 us (2%)
    all_gather x1, waiting for transfers between devices, body(): lax.all_gather(down_weight, 'sp', axis=1, tiled=True)  75.1 us
    all_gather x1, waiting for transfers between devices, body(): lax.all_gather(up_weight, 'sp', axis=0, tiled=True)  65.5 us
    reduce_scatter x1, waiting for transfers between devices, body(): lax.psum_scatter(head_terms.astype(jnp.bfloat16), 'tp', scatter_dimension...  56.4 us
    reduce_scatter x1, waiting for transfers between devices, body(): lax.psum_scatter(down_terms.astype(jnp.bfloat16), 'tp', scatter_dimension...  44.5 us
    dynamic_slice x48, local copies, waits for them, and re-layouts, block_pass(): lax.scan(advance, initial, (to_blocks(queries), to_blocks(keys_in), to_bl...  41.7 us
    all_gather x2, blocking collectives, entering(): lax.all_gather(a.astype(kind), axis)  39 us
    all_gather x1, waiting for transfers between devices, body(): normed = lax.all_gather(normed_cols, 'tp', axis=1, tiled=True)  34.1 us
    dot_general x32, matrix products, advance(): outside = jnp.einsum('ihd,hde->ihe', scaled_q, memory, precision=HIGHEST)  22.1 us
  transfers between devices with their start and end apart: 7, of which 6 were waited for; matrix products, arithmetic and copies ran while one was open for 24% of the time, Pallas kernels for 0%

commit v1 on v0

--- a/solution.py
+++ b/solution.py
@@ -125,7 +125,9 @@
 ):
     heads_here = HEADS // lax.axis_size("tp")
     up_whole, down_whole = (
-        lax.all_gather(up_weight, "sp", axis=0, tiled=True),
+        jnp.concatenate(
+            lax.all_to_all(jnp.stack([up_weight] * lax.axis_size("sp")), "sp", 0, 0), axis=0
+        ),
         lax.all_gather(down_weight, "sp", axis=1, tiled=True),
     )
     wq, wk, wv, wg = prepare(query_wide, key_wide, value_wide, decay_wide, heads_here)

time: 596 us -> 558 us (0.936)
  waiting for transfers between devices: 281 us -> 221 us
  starting transfers between devices: 0.47 us -> 18.7 us
    all_to_all x0 -> x1, waiting for transfers between devices: none -> 82.4 us  [body(): lax.all_to_all(jnp.stack([up_weight] * lax.axis_size('sp')), 'sp', 0, 0)]
    all_gather x1 -> x0, waiting for transfers between devices: 65.5 us -> none  [body(): lax.all_gather(up_weight, 'sp', axis=0, tiled=True)]
    all_gather x1, waiting for transfers between devices: 75.1 us -> 17.9 us  [body(): lax.all_gather(down_weight, 'sp', axis=1, tiled=True)]
    reduce_scatter x1, waiting for transfers between devices: 56.4 us -> 35.6 us  [body(): lax.psum_scatter(head_terms.astype(jnp.bfloat16), 'tp', scatter_dimension...]
    all_to_all x0 -> x1, starting transfers between devices: none -> 18.5 us  [body(): lax.all_to_all(jnp.stack([up_weight] * lax.axis_size('sp')), 'sp', 0, 0)]
  transfers between devices with their start and end apart: 7 -> 7, of which waited for: 6 -> 6; matrix products, arithmetic and copies ran while one was open for 24% -> 26% of each run, Pallas kernels for 0% -> 0%
where the time goes in v1:
time: 558 us; the launch traced here: 553 us
  waiting for transfers between devices  221 us (40%)
  matrix products  95.3 us (17%)
  local copies, waits for them, and re-layouts  85.9 us (15%)
  other arithmetic  71.2 us (13%)
  blocking collectives  45.1 us (8%)
  starting transfers between devices  18.7 us (3%)
  between operations  13.8 us (2%)
    all_to_all x1, waiting for transfers between devices, body(): lax.all_to_all(jnp.stack([up_weight] * lax.axis_size('sp')), 'sp', 0, 0)  82.4 us
    reduce_scatter x1, waiting for transfers between devices, body(): lax.psum_scatter(down_terms.astype(jnp.bfloat16), 'tp', scatter_dimension...  44.5 us
    dynamic_slice x48, local copies, waits for them, and re-layouts, block_pass(): lax.scan(advance, initial, (to_blocks(queries), to_blocks(keys_in), to_bl...  41.7 us
    all_gather x2, blocking collectives, entering(): lax.all_gather(a.astype(kind), axis)  39 us
    reduce_scatter x1, waiting for transfers between devices, body(): lax.psum_scatter(head_terms.astype(jnp.bfloat16), 'tp', scatter_dimension...  35.6 us
    all_gather x1, waiting for transfers between devices, body(): normed = lax.all_gather(normed_cols, 'tp', axis=1, tiled=True)  35.4 us
    dot_general x32, matrix products, advance(): outside = jnp.einsum('ihd,hde->ihe', scaled_q, memory, precision=HIGHEST)  22.1 us
    dot_general x32, matrix products, advance(): inside = jnp.einsum('hij,jhe->ihe', scores, block_v, precision=HIGHEST)  19.4 us
  transfers between devices with their start and end apart: 7, of which 6 were waited for; matrix products, arithmetic and copies ran while one was open for 26% of the time, Pallas kernels for 0%

profile of v1, /device:TPU:0, one launch (start us, length us, event | category | flops | bytes accessed | tf_op | source)
XLA Modules:
  0.0 552.9 jit_solution(9813216299249164384)
XLA Ops:
  6.6 5.0 reshape.507
  15.4 68.5 %while.51 = (s32[]{:T(128)}, f32[1,128,512]{2,1,0:T(8,128)S(1)}, f32[1,128]{1,0:T(1,128)S(1)}, f32[16,64,1,512]{3,1,2,0:T(8,128)}, f32[16,64,1,128]{3,1,2,0:T(8,...) while((s32[]{:T(128)}, f32[1,128,512]{2,1,0:T(8,128)S(1)}, ...), condition=%wide.region_5.6_spmd.clone, body=%wide.region_3.5_spmd.clone.sunk | while | flops 133005568 | bytes 2333321 | solution.py:65
  84.7 2.7 fusion.81
  87.3 3.3 reshape.491
  91.6 3.3 reshape.492
  94.9 4.9 reshape.505
  103.4 108.7 %while.50 = (s32[]{:T(128)}, f32[1,256,512]{2,1,0:T(8,128)S(1)}, f32[1,256]{1,0:T(1,128)S(1)}, f32[16,64,1,512]{3,1,2,0:T(8,128)}, f32[16,64,1,256]{3,1,2,0:T(8,...) while((s32[]{:T(128)}, f32[1,256,512]{2,1,0:T(8,128)S(1)}, ...), condition=%wide.region_2.3_spmd.clone, body=%wide.region_0.2_spmd.clone.sunk | while | flops 240787968 | bytes 3648133 | solution.py:65
  212.9 3.0 copy.32
  217.2 3.0 copy.34
  221.5 22.3 %all-gather.5 = bf16[8,1,128]{2,1,0:T(2,128)(2,1)S(1)} all-gather(bf16[1,1,128]{2,1,0:T(2,128)(2,1)S(1)} %convert_bitcast_fusion.1), channel_id=4, replica_groups=mesh['sp'=8,'tp'=4] {'sp'}, dimensions={0}, use_global_device_ids=true | all-gather | bytes 2304 | tf_op jit(solution)/shard_map/all_gather | solution.py:16
  243.9 16.7 %all-gather.4 = bf16[8,1,256]{2,1,0:T(2,128)(2,1)S(1)} all-gather(bf16[1,1,256]{2,1,0:T(2,128)(2,1)S(1)} %convert_bitcast_fusion), channel_id=2, replica_groups=mesh['sp'=8,'tp'=4] {'sp'}, dimensions={0}, use_global_device_ids=true | all-gather | bytes 4608 | tf_op jit(solution)/shard_map/all_gather | solution.py:16
  260.6 4.6 all-gather.15.cloned.1.call-done
  265.4 5.6 %multiply_reduce_fusion.1 = (f32[1024]{0:T(1024)S(1)}, f32[1024,1,512]{0,2,1:T(8,128)S(1)}) fusion(f32[1024,1,512]{0,2,1:T(8,128)} %copy.32, f32[1024,256]{1,0:T(8,128)} %bitcast.286, f32[1,256,512]{2,1,0:T(8,128)S(1)} %get-tuple-element.190), kind=kOutput, calls=%fused_computation.120 | convolution fusion | flops 1612184576 | bytes 5771264 | tf_op jit(solution)/shard_map/ihd,hde->ihe/dot_general | solution.py:146
  273.2 2.8 fusion.78
  276.0 5.0 add_convert_fusion
  282.1 2.5 stack.2
  284.5 18.5 %all-to-all-start = ((bf16[8,256,1024]{2,1,0:T(8,128)(2,1)}), bf16[8,256,1024]{2,1,0:T(8,128)(2,1)}, u32[]{:S(2)}, u32[]{:S(2)}) async-start(bf16[8,256,1024]{2,1,0:T(8,128)(2,1)} %stack.2), calls=%async_computation.1 | async-start | bytes 8388608 | tf_op jit(solution)/shard_map/all_to_all | solution.py:129
  303.9 35.6 %reduce-scatter.3.cloned.1.call-done = bf16[1024,512]{1,0:T(8,128)(2,1)} async-done(((bf16[1024,2048]{1,0:T(8,128)(2,1)}), bf16[1024,512]{1,0:T(8,128)(2,1)}) %reduce-scatter.3.cloned.1.call-update) | async-done | bytes 1048592 | tf_op jit(solution)/shard_map/reduce_scatter | solution.py:157
  341.4 6.1 %psum.7 = f32[1024,1]{0,1:T(1,128)S(1)} all-reduce(f32[1024,1]{0,1:T(1,128)S(1)} %bitcast.296), channel_id=1, replica_groups=mesh['sp'=8,'tp'=4] {'tp'}, use_global_device_ids=true, to_apply=%region_12.13 | all-reduce | flops 1024 | bytes 8192 | tf_op jit(solution)/shard_map/psum | solution.py:162
  348.9 82.4 %all-to-all-done = bf16[8,256,1024]{2,1,0:T(8,128)(2,1)} async-done(((bf16[8,256,1024]{2,1,0:T(8,128)(2,1)}), bf16[8,256,1024]{2,1,0:T(8,128)(2,1)}, u32[]{:S(2)}, u32[]{:S(2)}) %all-to-all-start) | async-done | bytes 4194336 | tf_op jit(solution)/shard_map/all_to_all | solution.py:129
  431.3 17.9 %all-gather.13.cloned.1.call-done = bf16[1024,2048]{1,0:T(8,128)(2,1)} async-done(((bf16[1024,256]{1,0:T(8,128)(2,1)}), bf16[1024,2048]{1,0:T(8,128)(2,1)}) %all-gather.13.cloned.1.call-update) | async-done | bytes 4194320 | tf_op jit(solution)/shard_map/all_gather | solution.py:131
  449.2 35.4 %all-gather.11.cloned.1.call-done = bf16[1024,2048]{1,0:T(8,128)(2,1)} async-done(((bf16[1024,512]{1,0:T(8,128)(2,1)}), bf16[1024,2048]{1,0:T(8,128)(2,1)}) %all-gather.11.cloned.1.call-update) | async-done | bytes 4194320 | tf_op jit(solution)/shard_map/all_gather | solution.py:167
  484.6 14.4 %convolution_convert_fusion = bf16[1024,2048]{1,0:T(8,128)(2,1)} fusion(bf16[1024,2048]{1,0:T(8,128)(2,1)} %all-gather.13.cloned.1.call-done, bf16[1024,2048]{1,0:T(8,128)(2,1)} %all-gather.11.cloned.1.call-done, bf16[2048,1024]{1,0:T(8,128)(2,1)} %bitcast.28), kind=kOutput, calls=%fused_computation.91 | convolution fusion | flops 8595177472 | bytes 16777216 | tf_op jit(solution)/shard_map/dot_general | solution.py:170
  499.0 44.5 %reduce-scatter.5.cloned.1.call-done = bf16[1024,512]{1,0:T(8,128)(2,1)} async-done(((bf16[1024,2048]{1,0:T(8,128)(2,1)}), bf16[1024,512]{1,0:T(8,128)(2,1)}) %reduce-scatter.5.cloned.1.call-update) | async-done | bytes 1048592 | tf_op jit(solution)/shard_map/reduce_scatter | solution.py:171
  (425 shorter events, 198.1 us)
Async XLA Ops:
  6.5 266.6 %copy-start = (bf16[512,2048]{1,0:T(8,128)(2,1)S(1)}, bf16[512,2048]{1,0:T(8,128)(2,1)}, u32[]{:S(2)}) copy-start(bf16[512,2048]{1,0:T(8,128)(2,1)} %param.35) | copy-start | bytes 6291460
  6.5 5.0 copy-start.11
  6.5 5.1 copy-start.12
  6.5 254.0 %all-gather.17.cloned.1.call-start = ((), (), s32[]{:S(2)}) async-start(), calls=%async_computation.8 | async-start | bytes 1179648 | tf_op jit(solution)/shard_map/all_gather | solution.py:16
  83.9 6.7 %copy-start.7 = (bf16[1024,256]{1,0:T(8,128)(2,1)S(1)}, bf16[1024,256]{1,0:T(8,128)(2,1)}, u32[]{:S(2)}) copy-start(bf16[1024,256]{1,0:T(8,128)(2,1)} %param.24) | copy-start | bytes 1572868
  84.6 180.5 %all-gather.15.cloned.1.call-start = ((), (), s32[]{:S(2)}) async-start(), calls=%async_computation.7 | async-start | bytes 2359296 | tf_op jit(solution)/shard_map/all_gather | solution.py:16
  94.9 4.9 copy-start.8
  212.9 126.6 %reduce-scatter.3.cloned.1.call-start = ((), (), s32[]{:S(2)}) async-start(), calls=%async_computation.3 | async-start | bytes 5242880 | tf_op jit(solution)/shard_map/reduce_scatter | solution.py:157
  212.9 3.0 copy-start.3
  217.2 3.0 copy-start.4
  265.4 5.7 %copy-start.2 = (f32[1024,1,512]{0,2,1:T(8,128)S(1)}, f32[1024,1,512]{0,2,1:T(8,128)}, u32[]{:S(2)}) copy-start(f32[1024,1,512]{0,2,1:T(8,128)} %copy.34) | copy-start | bytes 6291460
  265.4 5.7 %copy-start.10 = (f32[16,64,1,128]{3,1,2,0:T(8,128)S(1)}, f32[16,64,1,128]{3,1,2,0:T(8,128)}, u32[]{:S(2)}) copy-start(f32[16,64,1,128]{3,1,2,0:T(8,128)} %get-tuple-element.194) | copy-start | bytes 1572868
  271.1 2.1 copy-start.6
  271.1 2.1 copy-start.14
  273.2 2.8 copy-start.5
  273.2 2.8 copy-start.13
  281.0 1.0 copy-start.9
  281.0 168.2 %all-gather.13.cloned.1.call-start = ((), (), s32[]{:S(2)}) async-start(), calls=%async_computation.5 | async-start | bytes 4718592 | tf_op jit(solution)/shard_map/all_gather | solution.py:131
  284.5 146.8 %all-to-all-start = ((bf16[8,256,1024]{2,1,0:T(8,128)(2,1)}), bf16[8,256,1024]{2,1,0:T(8,128)(2,1)}, u32[]{:S(2)}, u32[]{:S(2)}) async-start(bf16[8,256,1024]{2,1,0:T(8,128)(2,1)} %stack.2), calls=%async_computation.1 | async-start | bytes 8388608 | tf_op jit(solution)/shard_map/all_to_all | solution.py:129
  303.0 181.6 %all-gather.11.cloned.1.call-start = ((), (), s32[]{:S(2)}) async-start(), calls=%async_computation.4 | async-start | bytes 5242880 | tf_op jit(solution)/shard_map/all_gather | solution.py:167
  348.8 194.7 %reduce-scatter.5.cloned.1.call-start = ((), (), s32[]{:S(2)}) async-start(), calls=%async_computation.6 | async-start | bytes 5242880 | tf_op jit(solution)/shard_map/reduce_scatter | solution.py:171
  499.0 47.0 %copy-start.1 = (bf16[512,2048]{1,0:T(8,128)(2,1)S(1)}, bf16[512,2048]{1,0:T(8,128)(2,1)}, u32[]{:S(2)}) copy-start(bf16[512,2048]{1,0:T(8,128)(2,1)} %param.35) | copy-start | bytes 6291460
Sparse Core Ops, SparseCore 0:
  84.7 43.0 all-gather.16
  213.0 52.1 all-gather.14
  281.2 58.2 reduce-scatter.2
  341.4 107.8 all-gather.12
  450.6 33.9 all-gather.10
  499.1 44.3 reduce-scatter.4
